TPU v7x, 256 devices: a whole 4x4x8 slice. The times are simulated.
256 devices in a mesh: ep: 128 (over z, y, x), tp: 2 (over core).
Axes of the slice: x: 4, y: 4, z: 8, core: 2. Of those that a mesh axis runs over, the one named last changes fastest.
Arguments:
- tokens: bfloat16 [2048, 2048], P('ep'), may hold values from -6 to 6
- recurrent_state: float32 [2048, 4, 128, 256], P('ep', 'tp'), may hold values from -6 to 6
- query_weight: bfloat16 [2048, 512], P(None, 'tp'), may hold values from -0.125 to 0.125
- key_weight: bfloat16 [2048, 512], P(None, 'tp'), may hold values from -0.125 to 0.125
- decay_weight: bfloat16 [2048, 512], P(None, 'tp'), may hold values from -0.5 to 0.5
- value_weight: bfloat16 [2048, 1024], P(None, 'tp'), may hold values from -0.125 to 0.125
- gate_weight: bfloat16 [2048, 1024], P(None, 'tp'), may hold values from -0.125 to 0.125
- head_gain: float32 [256], replicated, may hold values from 0.1 to 1.9
- output_weight: bfloat16 [1024, 2048], P('tp'), may hold values from -0.375 to 0.375
- norm_gain: float32 [2, 2048], replicated, may hold values from 0.1 to 1.9
- norm_bias: float32 [2, 2048], replicated, may hold values from -1.8 to 1.8
- group_router: bfloat16 [2048, 4], replicated, may hold values from -0.125 to 0.125
- router_weight: bfloat16 [2048, 256], replicated, may hold values from -0.125 to 0.125
- routes: int32 [2048, 2], P('ep'), may hold values from 0 to 255, as said below
- expert_gate: bfloat16 [256, 2048, 256], P(('ep', 'tp')), may hold values from -0.125 to 0.125
- expert_up: bfloat16 [256, 2048, 256], P(('ep', 'tp')), may hold values from -0.125 to 0.125
- expert_down: bfloat16 [256, 256, 2048], P(('ep', 'tp')), may hold values from -1.5 to 1.5
Outputs:
- new_tokens: bfloat16 [2048, 2048], P('ep', 'tp')
- new_state: float32 [2048, 4, 128, 256], P('ep', 'tp')
Inputs may be any that keep to these rules, and one draw needn't show every extreme that they name: `routes`: each row names two different experts of one group (group g holds the experts g * 64 to g * 64 + 63). In the rows of one device each group is named by the same number of rows and no expert by more than 2 rows; some expert is named by exactly 2 rows of every device.
All inputs are finite; a program needn't handle non-finite values.
Results may differ from a plain program's by a relative error of at most 0.01.
Values may be sent and summed in bfloat16 or wider, within the bound.
A program may use at most 128 MiB of HBM per device.

v0:
```python
import jax
import jax.numpy as jnp
from jax import lax
from jax.sharding import PartitionSpec as P

alpha_res = 2.0**0.5
eps_norm = 1e-05


def total_of_pieces(x, axis):
    return lax.all_gather(x, axis).astype(jnp.float32).sum(0)


def cut_along(x, dim, devices):
    before, after = (x.shape[:dim], x.shape[dim + 1 :])
    return jnp.moveaxis(x.reshape(*before, devices, -1, *after), dim, 0)


def joined_along(pieces, dim):
    shape = list(pieces.shape[1:])
    shape[dim] *= pieces.shape[0]
    return jnp.moveaxis(pieces, 0, dim).reshape(shape)


def joined_exchange(x, axis, axes, splits, concats):
    sizes = [lax.axis_size(a) for a in axes]
    pieces = cut_along(x, splits[0], sizes[0])
    pieces = jnp.moveaxis(cut_along(pieces, splits[1] + 1, sizes[1]), 0, 1)
    inside = pieces.shape[2:]
    pieces = pieces.reshape(-1, *inside)
    pieces = lax.all_to_all(pieces, axis, split_axis=0, concat_axis=0, tiled=True)
    pieces = joined_along(pieces.reshape(*sizes, *inside), concats[0] + 1)
    return joined_along(pieces, concats[1])


def layer_normed(inputs, gain_row, bias_row):
    centered = inputs - jnp.mean(inputs, axis=-1, keepdims=True)
    spread = jnp.mean(centered * centered, axis=-1, keepdims=True)
    return centered * lax.rsqrt(spread + eps_norm) * gain_row + bias_row


def on_device(
    tokens,
    recurrent_state,
    query_weight,
    key_weight,
    decay_weight,
    value_weight,
    gate_weight,
    head_gain,
    output_weight,
    norm_gain,
    norm_bias,
    group_router,
    router_weight,
    routes,
    expert_gate,
    expert_up,
    expert_down,
):
    row_count, model_width = tokens.shape
    heads_here = recurrent_state.shape[1]
    key_dim = recurrent_state.shape[2]
    value_dim = recurrent_state.shape[3]

    def project(weight):
        return jnp.dot(tokens, weight, preferred_element_type=jnp.float32)

    queries = project(query_weight).reshape(row_count, heads_here, key_dim) * key_dim ** (-0.5)
    key_rows = project(key_weight).reshape(row_count, heads_here, key_dim)
    value_rows = project(value_weight).reshape(row_count, heads_here, value_dim)
    gate_rows = project(gate_weight)
    decay_rate = jnp.exp(jax.nn.log_sigmoid(project(decay_weight)) / 16.0).reshape(
        row_count, heads_here, key_dim
    )
    new_state = (
        decay_rate[..., None] * recurrent_state + key_rows[..., None] * value_rows[:, :, None, :]
    )
    readout = jnp.sum(queries[..., None] * new_state, axis=2)
    norm_scale = lax.rsqrt(jnp.mean(readout * readout, axis=-1, keepdims=True) + eps_norm)
    gated_rows = (
        (readout * norm_scale * head_gain).reshape(row_count, heads_here * value_dim)
        * jax.nn.silu(gate_rows)
    ).astype(jnp.bfloat16)
    partial_value = jnp.dot(gated_rows, output_weight, preferred_element_type=jnp.float32)
    mixed_sum = total_of_pieces(partial_value.astype(jnp.bfloat16), "tp").astype(jnp.float32)
    hidden = layer_normed(
        alpha_res * tokens.astype(jnp.float32) + mixed_sum, norm_gain[0], norm_bias[0]
    ).astype(jnp.bfloat16)
    group_count = group_router.shape[1]
    expert_count = router_weight.shape[1]
    per_group = expert_count // group_count
    top_count = routes.shape[1]
    group_logit = jnp.dot(hidden, group_router, preferred_element_type=jnp.float32)
    expert_logit = jnp.dot(hidden, router_weight, preferred_element_type=jnp.float32)
    chosen_group = routes[:, 0] // per_group
    group_hit = chosen_group[:, None] == jnp.arange(group_count, dtype=jnp.int32)[None, :]
    own_logit = jnp.sum(jnp.where(group_hit, group_logit, 0.0), axis=1, keepdims=True)
    group_share = 1.0 / jnp.sum(jnp.exp(group_logit - own_logit), axis=1)
    expert_hit = routes[:, :, None] == jnp.arange(expert_count, dtype=jnp.int32)[None, None, :]
    picked = jnp.sum(jnp.where(expert_hit, expert_logit[:, None, :], 0.0), axis=2)
    route_weight = group_share[:, None] * jax.nn.sigmoid(picked - picked[:, ::-1])
    ep_count = lax.axis_size("ep")
    tp_count = lax.axis_size("tp")
    pair_index = lax.axis_index("tp")
    local_experts = expert_gate.shape[0]
    capacity = 2 * max(1, row_count // expert_count)
    total_slots = expert_count * capacity
    own_slots = total_slots // tp_count
    flat_routes = routes.reshape(row_count * top_count)
    onehot = (flat_routes[:, None] == jnp.arange(expert_count, dtype=jnp.int32)[None, :]).astype(
        jnp.int32
    )
    earlier_count = jnp.sum((jnp.cumsum(onehot, axis=0) - onehot) * onehot, axis=1)
    slot_index = flat_routes * capacity + earlier_count
    pick_all = (slot_index[:, None] == jnp.arange(total_slots, dtype=jnp.int32)[None, :]).astype(
        jnp.bfloat16
    )
    pick_mine = lax.dynamic_slice_in_dim(
        pick_all.reshape(row_count * top_count, ep_count, tp_count, local_experts * capacity),
        pair_index,
        1,
        2,
    ).reshape(row_count * top_count, own_slots)
    outgoing = jnp.einsum(
        "rks,rd->sd",
        pick_mine.reshape(row_count, top_count, own_slots),
        hidden,
        preferred_element_type=jnp.float32,
    ).astype(jnp.bfloat16)
    outgoing = outgoing.reshape(ep_count, local_experts, capacity, model_width)
    col_width = model_width // tp_count
    col_start = pair_index * col_width
    arrived = lax.all_to_all(outgoing, "ep", split_axis=0, concat_axis=0, tiled=True)
    gate_part = jnp.einsum(
        "secd,edf->secf", arrived, expert_gate, preferred_element_type=jnp.float32
    )
    up_part = jnp.einsum("secd,edf->secf", arrived, expert_up, preferred_element_type=jnp.float32)
    activation = (jax.nn.silu(gate_part) * up_part).astype(jnp.bfloat16)
    results = jnp.einsum(
        "secf,efd->secd", activation, expert_down, preferred_element_type=jnp.float32
    ).astype(jnp.bfloat16)
    returned = joined_exchange(results, ("ep", "tp"), ("ep", "tp"), (0, 3), (0, 1))
    fetched = jnp.dot(
        pick_all, returned.reshape(total_slots, col_width), preferred_element_type=jnp.float32
    ).reshape(row_count, top_count, col_width)
    routed_sum = jnp.sum(route_weight[..., None] * fetched, axis=1)
    blended = (
        alpha_res * lax.dynamic_slice_in_dim(hidden, col_start, col_width, 1).astype(jnp.float32)
        + routed_sum
    )
    row_total, row_squares = lax.psum(
        (jnp.sum(blended, axis=1), jnp.sum(blended * blended, axis=1)), "tp"
    )
    row_mean = row_total / model_width
    spread = row_squares / model_width - row_mean * row_mean
    gain_part = lax.dynamic_slice_in_dim(norm_gain[1], col_start, col_width, 0)
    shift_part = lax.dynamic_slice_in_dim(norm_bias[1], col_start, col_width, 0)
    new_tokens = (
        (blended - row_mean[:, None]) * lax.rsqrt(spread[:, None] + eps_norm) * gain_part
        + shift_part
    ).astype(jnp.bfloat16)
    return (new_tokens, new_state)


def solution(mesh):
    in_specs = (
        P("ep", None),
        P("ep", "tp", None, None),
        P(None, "tp"),
        P(None, "tp"),
        P(None, "tp"),
        P(None, "tp"),
        P(None, "tp"),
        P(),
        P("tp", None),
        P(),
        P(),
        P(),
        P(),
        P("ep", None),
        P(("ep", "tp"), None, None),
        P(("ep", "tp"), None, None),
        P(("ep", "tp"), None, None),
    )
    out_specs = (P("ep", "tp"), P("ep", "tp", None, None))
    return jax.shard_map(
        on_device, mesh=mesh, in_specs=in_specs, out_specs=out_specs, check_vma=False
    )
```

profile of v0, /device:TPU:1, one launch (start us, length us, event | category | flops | bytes accessed | tf_op | source)
XLA Modules:
  0.0 126.5 jit_solution(791586041143189918)
XLA Ops:
  0.7 0.9 fusion.37
  1.6 0.8 fusion.38
  2.4 0.8 copy.48
  3.6 1.5 %fusion.5 = f32[32,128,1,2]{3,1,0,2:T(8,128)} fusion(s32[128,1,2]{2,0,1:T(8,128)S(1)} %constant_dynamic-slice_fusion.1, s32[32]{0:T(128)S(1)} %multiply_add_fusion.5), kind=kLoop, calls=%fused_computation.16 | loop fusion | flops 24576 | bytes 33920 | tf_op jit(solution)/shard_map/rks,rd->sd/convert_element_type | solution.py:125
  5.1 2.8 %reshape.153 = f32[16,2,256]{2,1,0:T(2,128)S(1)} reshape(f32[32,128,1,2]{3,1,0,2:T(8,128)} %fusion.5) | data formatting | bytes 65536 | tf_op jit(solution)/shard_map/rks,rd->sd/convert_element_type | solution.py:125
  8.3 2.0 %fusion.42 = f32[16,512]{1,0:T(8,128)S(1)} fusion(bf16[16,2048]{1,0:T(8,128)(2,1)S(1)} %copy-done.1, bf16[2048,512]{1,0:T(8,128)(2,1)} %param.22), kind=kOutput, calls=%fused_computation.84 | convolution fusion | flops 33554432 | bytes 2195456 | tf_op jit(solution)/shard_map/dot_general | solution.py:67
  10.6 1.5 %fusion.30 = f32[16,256]{1,0:T(8,128)S(1)} fusion(bf16[16,2048]{1,0:T(8,128)(2,1)S(1)} %copy-done.1, bf16[2048,256]{1,0:T(8,128)(2,1)} %param.21), kind=kOutput, calls=%fused_computation.52 | convolution fusion | flops 16814080 | bytes 1130496 | tf_op jit(solution)/shard_map/dot_general | solution.py:67
  12.2 5.7 %multiply_reduce_fusion = (f32[16,2,256]{2,1,0:T(2,128)S(1)}, f32[16,2,128,256]{3,2,1,0:T(8,128)}) fusion(f32[16,2,128]{2,1,0:T(2,128)S(1)} %mul.188, f32[16,2,256]{2,1,0:T(2,128)S(1)} %mul.195, f32[16,2,128]{2,1,0:T(2,128)S(1)} %mul.193, f32[16,2,128,256]{3,2,1,0:T(8,128)} %param.18, f32[16,2,128]{2,1,0:T(2,128)S(1)} %mul.190), kind=kLoop, calls=%fused_computation | loop fusion | flops 5234688 | bytes 8503296 | tf_op jit(solution)/shard_map/reduce_sum | solution.py:79
  18.1 2.3 %convolution_convert_fusion.2 = bf16[16,2048]{1,0:T(8,128)(2,1)S(1)} fusion(bf16[512,2048]{1,0:T(8,128)(2,1)S(1)} %copy-done, f32[16,512]{1,0:T(8,128)S(1)} %bitcast.110, f32[512]{0:T(512)S(1)} %bitcast.116, bf16[16,2048]{1,0:T(8,128)(2,1)S(1)} %copy-done.1, bf16[2048,512]{1,0:T(8,128)(2,1)} %param.23), kind=kOutput, calls=%fused_computation.5 | convolution fusion | flops 67198976 | bytes 4360192 | tf_op jit(solution)/shard_map/dot_general | solution.py:85
  20.4 4.7 %all-gather = bf16[32,2048]{1,0:T(8,128)(2,1)S(1)} all-gather(bf16[16,2048]{1,0:T(8,128)(2,1)S(1)} %convolution_convert_fusion.2), channel_id=2, replica_groups=mesh['ep'=128,'tp'=2] {'tp'}, dimensions={0}, use_global_device_ids=true | all-gather | bytes 196608 | tf_op jit(solution)/shard_map/all_gather | solution.py:11
  25.7 0.4 fusion.44
  26.2 1.5 %reshape.144 = bf16[128,1,2,2048]{3,2,0,1:T(2,128)(2,1)} reshape(bf16[256,2048]{1,0:T(8,128)(2,1)S(1)} %fusion.44) | data formatting | bytes 2097152 | tf_op jit(solution)/shard_map/reshape | solution.py:131
  27.7 43.1 %all_to_all.10 = bf16[128,1,2,2048]{3,2,1,0:T(2,128)(2,1)S(1)} all-to-all(bf16[128,1,2,2048]{3,2,1,0:T(2,128)(2,1)} %bitcast.107), channel_id=1, replica_groups=mesh['ep'=128,'tp'=2] {'ep'}, dimensions={0} | all-to-all | bytes 2097152 | tf_op jit(solution)/shard_map/all_to_all | solution.py:134
  70.7 1.4 %convolution_bitcast_fusion.1 = f32[128,1,2,256]{3,0,2,1:T(8,128)} fusion(bf16[1,2048,256]{2,1,0:T(8,128)(2,1)S(1)} %copy-done.6, bf16[128,1,2,2048]{3,2,1,0:T(2,128)(2,1)S(1)} %all_to_all.10), kind=kOutput, calls=%fused_computation.9 | convolution fusion | flops 268435456 | bytes 2359296 | tf_op jit(solution)/shard_map/secd,edf->secf/dot_general | solution.py:135
  72.2 3.9 %fusion = bf16[128,1,2,2048]{3,0,2,1:T(8,128)(2,1)} fusion(bf16[1,256,2048]{2,1,0:T(8,128)(2,1)} %param.33, bf16[1,2048,256]{2,1,0:T(8,128)(2,1)} %param.32, bf16[128,1,2,2048]{3,2,1,0:T(2,128)(2,1)S(1)} %all_to_all.10, f32[128,1,2,256]{3,0,2,1:T(8,128)} %convolution_bitcast_fusion.1), kind=kOutput, calls=%fused_computation.4 | convolution fusion | flops 537788416 | bytes 4456448 | tf_op jit(solution)/shard_map/secf,efd->secd/dot_general | solution.py:140
  76.1 1.8 %reshape_reshape.7 = bf16[128,1,1,2,2,1024]{5,4,0,3,2,1:T(2,128)(2,1)S(1)} reshape(bf16[128,1,2,2048]{3,0,2,1:T(8,128)(2,1)} %fusion) | data formatting | bytes 2097152 | tf_op jit(solution)/shard_map/reshape;reshape | solution.py:16
  77.9 2.6 %copy.52 = bf16[128,2,1,1,2,1024]{5,4,1,0,3,2:T(2,128)(2,1)} copy(bf16[128,2,1,1,2,1024]{5,1,0,4,3,2:T(2,128)(2,1)S(1)} %bitcast.108) | data formatting | bytes 2097152 | tf_op jit(solution)/shard_map/transpose;transpose | solution.py:28
  80.5 8.2 %all-to-all-start.1 = ((bf16[256,1,1,2,1024]{4,3,2,1,0:T(2,128)(2,1)}), bf16[256,1,1,2,1024]{4,3,2,1,0:T(2,128)(2,1)S(1)}, u32[]{:S(2)}, u32[]{:S(2)}) async-start(bf16[256,1,1,2,1024]{4,3,2,1,0:T(2,128)(2,1)} %bitcast.106), calls=%async_computation.1 | async-start | bytes 2097152 | tf_op jit(solution)/shard_map/all_to_all | solution.py:31
  88.8 1.5 %fusion.43 = f32[16,256]{1,0:T(8,128)S(1)} fusion(bf16[16,2048]{1,0:T(8,128)(2,1)S(1)} %add_convert_fusion, bf16[2048,256]{1,0:T(8,128)(2,1)} %param.29), kind=kOutput, calls=%fused_computation.85 | convolution fusion | flops 16777216 | bytes 1130496 | tf_op jit(solution)/shard_map/dot_general | solution.py:95
  90.9 28.3 %all-to-all-done.1 = bf16[256,1,1,2,1024]{4,3,2,1,0:T(2,128)(2,1)S(1)} async-done(((bf16[256,1,1,2,1024]{4,3,2,1,0:T(2,128)(2,1)}), bf16[256,1,1,2,1024]{4,3,2,1,0:T(2,128)(2,1)S(1)}, u32[]{:S(2)}, u32[]{:S(2)}) %all-to-all-start.1) | async-done | bytes 1048608 | tf_op jit(solution)/shard_map/all_to_all | solution.py:31
  119.1 1.2 reshape.159
  120.3 1.5 %fusion.4 = f32[16,1024]{1,0:T(8,128)S(1)} fusion(bf16[512,1024,1]{1,0,2:T(8,128)(2,1)} %reshape.159, f32[16,2]{0,1:T(2,128)S(1)} %divide_multiply_fusion, s32[16,2]{0,1:T(2,128)S(1)} %multiply_add_fusion.4), kind=kOutput, calls=%fused_computation.13 | convolution fusion | flops 33619968 | bytes 1114368 | tf_op jit(solution)/shard_map/dot_general | solution.py:144
  122.0 3.8 %all-reduce = (f32[16]{0:T(128)S(1)}, f32[16]{0:T(128)S(1)}) all-reduce(f32[16]{0:T(128)S(1)} %get-tuple-element.3, f32[16]{0:T(128)S(1)} %get-tuple-element.2), channel_id=1, replica_groups=mesh['ep'=128,'tp'=2] {'tp'}, use_global_device_ids=true, to_apply=%region_15.16 | all-reduce | flops 32 | bytes 256 | tf_op jit(solution)/shard_map/psum | solution.py:152
  125.8 0.7 add_convert_fusion.1
  (55 shorter events, 2.5 us)
Async XLA Ops:
  0.6 17.5 %copy-start = (bf16[512,2048]{1,0:T(8,128)(2,1)S(1)}, bf16[512,2048]{1,0:T(8,128)(2,1)}, u32[]{:S(2)}) copy-start(bf16[512,2048]{1,0:T(8,128)(2,1)} %param.25) | copy-start | bytes 6291460
  3.6 4.4 %copy-start.1 = (bf16[16,2048]{1,0:T(8,128)(2,1)S(1)}, bf16[16,2048]{1,0:T(8,128)(2,1)}, u32[]{:S(2)}) copy-start(bf16[16,2048]{1,0:T(8,128)(2,1)} %param.17) | copy-start | bytes 196612
  3.6 4.4 %copy-start.2 = (bf16[2048,256]{1,0:T(8,128)(2,1)S(1)}, bf16[2048,256]{1,0:T(8,128)(2,1)}, u32[]{:S(2)}) copy-start(bf16[2048,256]{1,0:T(8,128)(2,1)} %param.19) | copy-start | bytes 3145732
  8.2 2.1 %copy-start.3 = (bf16[2048,256]{1,0:T(8,128)(2,1)S(1)}, bf16[2048,256]{1,0:T(8,128)(2,1)}, u32[]{:S(2)}) copy-start(bf16[2048,256]{1,0:T(8,128)(2,1)} %param.20) | copy-start | bytes 3145732
  12.2 5.9 %copy-start.5 = (f32[256]{0:T(256)S(1)}, f32[256]{0:T(256)}, u32[]{:S(2)}) copy-start(f32[256]{0:T(256)} %param.24) | copy-start | bytes 3076
  27.7 43.1 %copy-start.6 = (bf16[1,2048,256]{2,1,0:T(8,128)(2,1)S(1)}, bf16[1,2048,256]{2,1,0:T(8,128)(2,1)}, u32[]{:S(2)}) copy-start(bf16[1,2048,256]{2,1,0:T(8,128)(2,1)} %param.31) | copy-start | bytes 3145732
  80.5 9.8 %copy-start.4 = (s32[16,2]{0,1:T(2,128)S(1)}, s32[16,2]{0,1:T(2,128)}, u32[]{:S(2)}) copy-start(s32[16,2]{0,1:T(2,128)} %param.30) | copy-start | bytes 388
  80.5 10.1 %copy-start.7 = (bf16[2048,4]{0,1:T(4,128)(2,1)S(1)}, bf16[2048,4]{0,1:T(4,128)(2,1)}, u32[]{:S(2)}) copy-start(bf16[2048,4]{0,1:T(4,128)(2,1)} %param.28) | copy-start | bytes 49156
  80.5 38.6 %all-to-all-start.1 = ((bf16[256,1,1,2,1024]{4,3,2,1,0:T(2,128)(2,1)}), bf16[256,1,1,2,1024]{4,3,2,1,0:T(2,128)(2,1)S(1)}, u32[]{:S(2)}, u32[]{:S(2)}) async-start(bf16[256,1,1,2,1024]{4,3,2,1,0:T(2,128)(2,1)} %bitcast.106), calls=%async_computation.1 | async-start | bytes 2097152 | tf_op jit(solution)/shard_map/all_to_all | solution.py:31
where the time goes:
time: 127 us
  blocking collectives  51.6 us (41%)
  waiting for transfers between devices  28.3 us (22%)
  matrix products  15.4 us (12%)
  local copies, waits for them, and re-layouts  12.9 us (10%)
  other arithmetic  9.27 us (7%)
  starting transfers between devices  8.22 us (6%)
    all_to_all x1, blocking collectives, on_device(): lax.all_to_all(outgoing, 'ep', split_axis=0, concat_axis=0, tiled=True)  43.1 us
    all_to_all x1, waiting for transfers between devices, joined_exchange(): lax.all_to_all(pieces, axis, split_axis=0, concat_axis=0, tiled=True)  28.3 us
    all_to_all x1, starting transfers between devices, joined_exchange(): lax.all_to_all(pieces, axis, split_axis=0, concat_axis=0, tiled=True)  8.22 us
    reduce_sum x1, other arithmetic, on_device(): readout = jnp.sum(queries[..., None] * new_state, axis=2)  5.65 us
    all_gather x1, blocking collectives, total_of_pieces(): return lax.all_gather(x, axis).astype(jnp.float32).sum(0)  4.74 us
    dot_general x4, matrix products, project(): return jnp.dot(tokens, weight, preferred_element_type=jnp.float32)  4.04 us
    dot_general x1, matrix products, on_device(): jnp.einsum('secf,efd->secd', activation, expert_down, preferred_element_t...  3.91 us
    psum x1, blocking collectives, on_device(): lax.psum((jnp.sum(blended, axis=1), jnp.sum(blended * blended, axis=1)),...  3.81 us
  transfers between devices with their start and end apart: 1, of which 1 were waited for; matrix products, arithmetic and copies ran while one was open for 2% of the time, Pallas kernels for 0%

commit v1 on v0

v1 whole, which is shorter than its diff:
```python
import functools

import jax
import jax.numpy as jnp
from jax import lax
from jax.experimental import pallas as pl
from jax.experimental.pallas import tpu as pltpu
from jax.sharding import PartitionSpec as P

MESH = pl.DeviceIdType.MESH
BF16 = jnp.bfloat16
F32 = jnp.float32
ROOT2 = 2.0**0.5
EPS = 1e-05

NX, NY, NZ = 4, 4, 8
ROWS = 16
WIDTH = 2048
HALF = 1024
CARRY = HALF + 128
FOLD = 256
SLAB = FOLD + 128
OFF = (0, 1, -1, 2)
OFFZ = (0, 1, -1, 2, -2, 3, -3, 4)
VIA_PLUS = (0, 3)
VIA_MINUS = (1, 2)
NCOPY = 128


def iota(shape, dim):
    return lax.broadcasted_iota(jnp.int32, shape, dim)


def where_bf16(mask):
    return jnp.where(mask, 1.0, 0.0).astype(BF16)


def dotf(a, b):
    return jnp.dot(a, b, preferred_element_type=F32)


def moe_kernel(
    gated_ref,
    tokens_ref,
    gain_ref,
    bias_ref,
    group_ref,
    routes_ref,
    wo_hbm,
    router_hbm,
    gate_hbm,
    up_hbm,
    down_hbm,
    out_ref,
    wo_v,
    router_v,
    gate_v,
    up_v,
    down_v,
    xs,
    xr,
    hid,
    zs,
    zr,
    own,
    part,
    ps,
    pr,
    red,
    fwd_in,
    top_in,
    low_in,
    low_out,
    fin,
    zback,
    zret,
    st_s,
    st_r,
    local_sem,
    send_sem,
    recv_sem,
):
    ep = lax.axis_index("ep")
    core = lax.axis_index("tp")
    x = lax.rem(ep, NX)
    y = lax.rem(ep // NX, NY)
    z = ep // (NX * NY)

    def device(dx=0, dy=0, dz=0, flip=False):
        ex = lax.rem(x + (dx + NX), NX)
        ey = lax.rem(y + (dy + NY), NY)
        ez = lax.rem(z + (dz + NZ), NZ)
        return {"ep": (ez * NY + ey) * NX + ex, "tp": (1 - core) if flip else core}

    def along(first, step):
        return device(dx=step) if first else device(dy=step)

    pair = device(flip=True)
    peers = [pair]
    peers += [device(dz=d) for d in OFFZ[1:]]
    peers += [device(dx=d) for d in OFF[1:]]
    peers += [device(dy=d) for d in OFF[1:]]
    barrier = pltpu.get_barrier_semaphore()
    for peer in peers:
        pl.semaphore_signal(barrier, inc=1, device_id=peer, device_id_type=MESH)

    loads = []
    for n, (src, dst) in enumerate(
        (
            (wo_hbm, wo_v),
            (router_hbm, router_v),
            (gate_hbm.at[0], gate_v),
            (up_hbm.at[0], up_v),
            (down_hbm.at[0], down_v),
        )
    ):
        load = pltpu.make_async_copy(src, dst, local_sem.at[n])
        load.start()
        loads.append(load)

    made = []

    def send(src, dst, to):
        n = len(made)
        copy = pltpu.make_async_remote_copy(
            src_ref=src,
            dst_ref=dst,
            send_sem=send_sem.at[n],
            recv_sem=recv_sem.at[n],
            device_id=to,
            device_id_type=MESH,
        )
        copy.start()
        made.append(copy)
        return copy

    loads[0].wait()
    partial_bf = dotf(gated_ref[...], wo_v[...]).astype(BF16)
    xs[...] = partial_bf
    pl.semaphore_wait(barrier, len(peers))
    exchange = send(xs, xr, pair)
    mixed = ROOT2 * tokens_ref[...].astype(F32) + partial_bf.astype(F32)

    routes = routes_ref[...]
    first_route, second_route = routes[:, 0:1], routes[:, 1:2]
    group_col = lax.shift_right_logical(first_route, 6)
    lanes = iota((ROWS, 128), 1)
    onehot_group = where_bf16(lanes == group_col)
    lower = where_bf16(iota((ROWS, ROWS), 0) > iota((ROWS, ROWS), 1))
    earlier = dotf(lower, onehot_group)
    rank_col = jnp.sum(jnp.where(lanes == group_col, earlier, 0.0), axis=1, keepdims=True)
    place_col = group_col.astype(F32) * 4.0 + rank_col
    diagonal = jnp.where(iota((ROWS, ROWS), 0) == iota((ROWS, ROWS), 1), place_col, 0.0)
    place_row = dotf(jnp.ones((64, ROWS), BF16), diagonal.astype(BF16))
    slab_row = iota((64, ROWS), 0)
    wanted = ((slab_row >> 4) * 4 + (slab_row & 3)).astype(F32)
    quarter = (slab_row >> 2) & 3
    match = place_row == wanted

    exchange.wait_recv()
    mixed = mixed + xr[...].astype(F32)
    mean = jnp.mean(mixed, axis=-1, keepdims=True)
    centered = mixed - mean
    spread = jnp.mean(centered * centered, axis=-1, keepdims=True)
    hidden = (
        centered * lax.rsqrt(spread + EPS) * gain_ref[0:1, :] + bias_ref[0:1, :]
    ).astype(BF16)
    hid[...] = hidden

    loads[1].wait()
    expert_logit = dotf(hidden, router_v[...])
    hidden_f = hidden.astype(F32)
    group_logit = [
        jnp.sum(hidden_f * group_ref[g : g + 1, :].astype(F32), axis=1, keepdims=True)
        for g in range(4)
    ]
    own_logit = jnp.zeros_like(group_logit[0])
    for g in range(4):
        own_logit = own_logit + jnp.where(group_col == g, group_logit[g], 0.0)
    share_sum = jnp.zeros_like(own_logit)
    for g in range(4):
        share_sum = share_sum + jnp.exp(group_logit[g] - own_logit)
    share = 1.0 / share_sum
    wide = iota((ROWS, 256), 1)
    picked0 = jnp.sum(jnp.where(wide == first_route, expert_logit, 0.0), axis=1, keepdims=True)
    picked1 = jnp.sum(jnp.where(wide == second_route, expert_logit, 0.0), axis=1, keepdims=True)
    weight0 = share * jax.nn.sigmoid(picked0 - picked1)
    weight1 = share * jax.nn.sigmoid(picked1 - picked0)
    meta = (
        jnp.where(lanes == (first_route & 63), weight0, 0.0)
        + jnp.where(lanes == (second_route & 63), weight1, 0.0)
    ).astype(BF16)

    my_cols = pl.multiple_of(core * HALF, HALF)
    other_cols = pl.multiple_of((1 - core) * HALF, HALF)
    slabs = jnp.zeros((64, FOLD), F32)
    for q in range(4):
        pick = where_bf16(match & (quarter == q))
        slabs = slabs + dotf(pick, hid[:, pl.ds(pl.multiple_of(my_cols + q * FOLD, FOLD), FOLD)])
    slab_meta = dotf(where_bf16(match & (quarter == 0)), meta)
    zs[:, :, 0:FOLD] = slabs.astype(BF16).reshape(4, 16, FOLD)
    zs[:, :, FOLD:SLAB] = slab_meta.astype(BF16).reshape(4, 16, 128)
    z_sends = [None]
    for k in range(1, NZ):
        to_z = lax.rem(z + (OFFZ[k] + NZ), NZ)
        z_sends.append(send(zs.at[to_z // 2], zr.at[k], device(dz=OFFZ[k])))
    zr[0] = zs[z // 2]

    out_i = iota((64, 64), 0)
    in_i = iota((64, 64), 1)
    unfold = where_bf16(
        in_i == ((out_i >> 2) & 3) * 16 + (out_i >> 4) * 4 + (out_i & 3)
    )

    def slot(i, h, j):
        return i * 8 + h * 4 + j

    arrive = {}

    def p1_sends(h):
        for j in (3, 1, 2):
            arrive[0, h, j] = send(
                own.at[slot(0, h, 0)], own.at[slot(0, h, j)], along(h == 0, OFF[j])
            )

    def p2_sends(h, j):
        for i in (1, 2):
            arrive[i, h, j] = send(
                own.at[slot(0, h, j)], own.at[slot(i, h, j)], along(h == 1, OFF[i])
            )

    def forward(h, j):
        i = 1 if j in VIA_PLUS else 2
        arrive[i, h, j].wait_recv()
        arrive[3, h, j] = send(
            own.at[slot(i, h, j)], own.at[slot(3, h, j)], along(h == 1, OFF[i])
        )

    def to_pair(first, count):
        return send(
            own.at[pl.ds(first, count), :, pl.ds(0, HALF)],
            part.at[pl.ds(first, count)],
            pair,
        )

    for h in range(2):
        for k in range(4 * h, 4 * h + 4):
            if k:
                z_sends[k].wait_recv()
        block = dotf(unfold, zr[4 * h : 4 * h + 4].reshape(64, SLAB)).astype(BF16)
        for q in range(4):
            own[slot(0, h, 0), :, q * FOLD : (q + 1) * FOLD] = block[
                q * 16 : (q + 1) * 16, 0:FOLD
            ]
        own[slot(0, h, 0), :, HALF:CARRY] = block[0:16, FOLD:SLAB]
        p1_sends(h)
        p2_sends(h, 0)

    half_copies = {}
    for h in range(2):
        for j in (1, 2, 3):
            arrive[0, h, j].wait_recv()
            p2_sends(h, j)
        half_copies[0, h] = to_pair(slot(0, h, 0), 4)
    for j in (0, 1, 2, 3):
        for h in range(2):
            forward(h, j)

    my_expert = lax.rem(ep, 32) * 2 + core

    for load in loads[2:]:
        load.wait()

    def experts(i, count):
        rows = count * 128
        first = i * 8
        mine = own[first : first + count * 8, :, 0:HALF].reshape(rows, HALF)
        theirs = part[first : first + count * 8].reshape(rows, HALF)
        marks = own[first : first + count * 8, :, HALF:CARRY].reshape(rows, 128).astype(F32)
        weight = jnp.sum(
            jnp.where(iota((rows, 128), 1) == my_expert, marks, 0.0), axis=1, keepdims=True
        )
        my_rows, other_rows = pl.ds(my_cols, HALF), pl.ds(other_cols, HALF)
        gate = dotf(mine, gate_v[my_rows, :]) + dotf(theirs, gate_v[other_rows, :])
        up = dotf(mine, up_v[my_rows, :]) + dotf(theirs, up_v[other_rows, :])
        act = (jax.nn.silu(gate) * up).astype(BF16)
        away = dotf(act, down_v[:, pl.ds(other_cols, HALF)]) * weight
        ps[first : first + count * 8] = away.astype(BF16).reshape(count * 8, 16, HALF)
        copy = send(
            ps.at[pl.ds(first, count * 8)], pr.at[pl.ds(first, count * 8)], pair
        )
        here = dotf(act, down_v[:, pl.ds(my_cols, HALF)]) * weight
        red[first : first + count * 8] = here.astype(BF16).reshape(count * 8, 16, HALF)
        return copy

    def add_pair(copy, i, count):
        copy.wait_recv()
        span = slice(i * 8, (i + count) * 8)
        red[span] = (red[span].astype(F32) + pr[span].astype(F32)).astype(BF16)

    for h in range(2):
        half_copies[0, h].wait_recv()
    result0 = experts(0, 1)

    for i in (1, 2):
        for h in range(2):
            for j in range(4):
                if (i == 1) != (j in VIA_PLUS):
                    arrive[i, h, j].wait_recv()
    middle = to_pair(8, 16)
    add_pair(result0, 0, 1)
    middle.wait_recv()
    result1 = experts(1, 2)
    for h in range(2):
        for j in range(4):
            arrive[3, h, j].wait_recv()
    last = to_pair(24, 8)
    add_pair(result1, 1, 2)

    top = {}

    def top_send(i, h, j):
        top[i, h, j] = send(
            red.at[slot(i, h, j)],
            top_in.at[(i - 1) * 8 + h * 4 + j],
            along(h == 1, -OFF[i]),
        )

    for h in range(2):
        for j in VIA_MINUS:
            top_send(1, h, j)
        for j in VIA_PLUS:
            top_send(2, h, j)
    last.wait_recv()
    result2 = experts(3, 1)
    add_pair(result2, 3, 1)
    back = {}
    for h in range(2):
        for j in range(4):
            i = 1 if j in VIA_PLUS else 2
            back[h, j] = send(
                red.at[slot(3, h, j)], fwd_in.at[h * 4 + j], along(h == 1, -OFF[i])
            )
    for h in range(2):
        for j in range(4):
            i = 1 if j in VIA_PLUS else 2
            back[h, j].wait_recv()
            s = slot(i, h, j)
            red[s] = (red[s].astype(F32) + fwd_in[h * 4 + j].astype(F32)).astype(BF16)
            top_send(i, h, j)
    low = {}
    for j in (3, 1, 2, 0):
        for h in range(2):
            total = red[slot(0, h, j)].astype(F32)
            for i in (1, 2):
                top[i, h, j].wait_recv()
                total = total + top_in[(i - 1) * 8 + h * 4 + j].astype(F32)
            if j:
                low_out[h * 4 + j] = total.astype(BF16)
                low[h, j] = send(
                    low_out.at[h * 4 + j], low_in.at[h * 4 + j], along(h == 0, -OFF[j])
                )
            else:
                fin[h] = total

    fold_i = iota((64, 16), 0)
    fold_o = iota((64, 16), 1)
    fold_match = fold_o == (fold_i >> 4) * 4 + (fold_i & 3)
    fold_quarter = (fold_i >> 2) & 3
    z_back = [None]
    for h in range(2):
        total = fin[h]
        for j in (1, 2, 3):
            low[h, j].wait_recv()
            total = total + low_in[h * 4 + j].astype(F32)
        total = total.astype(BF16)
        folded = jnp.zeros((64, FOLD), F32)
        for q in range(4):
            folded = folded + dotf(
                where_bf16(fold_match & (fold_quarter == q)),
                total[:, q * FOLD : (q + 1) * FOLD],
            )
        zback[4 * h : 4 * h + 4] = folded.astype(BF16).reshape(4, 16, FOLD)
        for k in range(4 * h, 4 * h + 4):
            if k:
                z_back.append(send(zback.at[k], zret.at[k], device(dz=-OFFZ[k])))
    zret[0] = zback[0]

    take_o = iota((64, 128), 0)
    take_i = iota((64, 128), 1)
    slab_k = take_i >> 4
    away_k = (slab_k + 1) >> 1
    signed = jnp.where((slab_k & 1) == 1, away_k, -away_k)
    plane = (z + signed + NZ) & (NZ - 1)
    expected = ((plane >> 1) * 4 + (take_i & 3)).astype(F32)
    place_tall = jnp.concatenate([place_col] * 4, axis=0)
    take = where_bf16(
        (expected == place_tall) & ((take_o >> 4) == ((take_i >> 2) & 3))
    )
    for k in range(1, NZ):
        z_back[k].wait_recv()
    routed = dotf(take, zret[...].reshape(128, FOLD))
    routed = jnp.concatenate([routed[q * 16 : (q + 1) * 16] for q in range(4)], axis=1)
    blended = ROOT2 * hid[:, pl.ds(my_cols, HALF)].astype(F32) + routed
    row_sum = jnp.sum(blended, axis=1, keepdims=True)
    row_sq = jnp.sum(blended * blended, axis=1, keepdims=True)
    st_s[...] = jnp.where(lanes == 0, row_sum, row_sq)
    stats = send(st_s, st_r, pair)
    stats.wait_recv()
    row_mean = (row_sum + st_r[:, 0:1]) / WIDTH
    spread = (row_sq + st_r[:, 1:2]) / WIDTH - row_mean * row_mean
    out_ref[...] = (
        (blended - row_mean)
        * lax.rsqrt(spread + EPS)
        * gain_ref[1:2, pl.ds(my_cols, HALF)]
        + bias_ref[1:2, pl.ds(my_cols, HALF)]
    ).astype(BF16)
    for copy in made:
        copy.wait_send()


def moe(gated, tokens, gain, bias, group_rows, routes, wo, router, gate, up, down):
    vmem = pl.BlockSpec(memory_space=pltpu.VMEM)
    anywhere = pl.BlockSpec(memory_space=pl.ANY)
    return pl.pallas_call(
        moe_kernel,
        out_shape=jax.ShapeDtypeStruct((ROWS, HALF), BF16),
        in_specs=[vmem] * 6 + [anywhere] * 5,
        out_specs=vmem,
        scratch_shapes=[
            pltpu.VMEM((512, WIDTH), BF16),
            pltpu.VMEM((WIDTH, 256), BF16),
            pltpu.VMEM((WIDTH, 256), BF16),
            pltpu.VMEM((WIDTH, 256), BF16),
            pltpu.VMEM((256, WIDTH), BF16),
            pltpu.VMEM((ROWS, WIDTH), BF16),
            pltpu.VMEM((ROWS, WIDTH), BF16),
            pltpu.VMEM((ROWS, WIDTH), BF16),
            pltpu.VMEM((4, 16, SLAB), BF16),
            pltpu.VMEM((8, 16, SLAB), BF16),
            pltpu.VMEM((32, 16, CARRY), BF16),
            pltpu.VMEM((32, 16, HALF), BF16),
            pltpu.VMEM((32, 16, HALF), BF16),
            pltpu.VMEM((32, 16, HALF), BF16),
            pltpu.VMEM((32, 16, HALF), BF16),
            pltpu.VMEM((8, 16, HALF), BF16),
            pltpu.VMEM((16, 16, HALF), BF16),
            pltpu.VMEM((8, 16, HALF), BF16),
            pltpu.VMEM((8, 16, HALF), BF16),
            pltpu.VMEM((2, 16, HALF), F32),
            pltpu.VMEM((8, 16, FOLD), BF16),
            pltpu.VMEM((8, 16, FOLD), BF16),
            pltpu.VMEM((ROWS, 128), F32),
            pltpu.VMEM((ROWS, 128), F32),
            pltpu.SemaphoreType.DMA((5,)),
            pltpu.SemaphoreType.DMA((NCOPY,)),
            pltpu.SemaphoreType.DMA((NCOPY,)),
        ],
        compiler_params=pltpu.CompilerParams(
            collective_id=0, has_side_effects=True, vmem_limit_bytes=40 * 1024 * 1024
        ),
        name="route_and_experts",
    )(gated, tokens, gain, bias, group_rows, routes, wo, router, gate, up, down)


def on_device(
    tokens,
    recurrent_state,
    query_weight,
    key_weight,
    decay_weight,
    value_weight,
    gate_weight,
    head_gain,
    output_weight,
    norm_gain,
    norm_bias,
    group_router,
    router_weight,
    routes,
    expert_gate,
    expert_up,
    expert_down,
):
    row_count, model_width = tokens.shape
    heads_here = recurrent_state.shape[1]
    key_dim = recurrent_state.shape[2]
    value_dim = recurrent_state.shape[3]

    def project(weight):
        return jnp.dot(tokens, weight, preferred_element_type=jnp.float32)

    queries = project(query_weight).reshape(row_count, heads_here, key_dim) * key_dim ** (-0.5)
    key_rows = project(key_weight).reshape(row_count, heads_here, key_dim)
    value_rows = project(value_weight).reshape(row_count, heads_here, value_dim)
    gate_rows = project(gate_weight)
    decay_rate = jnp.exp(jax.nn.log_sigmoid(project(decay_weight)) / 16.0).reshape(
        row_count, heads_here, key_dim
    )
    new_state = (
        decay_rate[..., None] * recurrent_state + key_rows[..., None] * value_rows[:, :, None, :]
    )
    readout = jnp.sum(queries[..., None] * new_state, axis=2)
    norm_scale = lax.rsqrt(jnp.mean(readout * readout, axis=-1, keepdims=True) + EPS)
    gated_rows = (
        (readout * norm_scale * head_gain).reshape(row_count, heads_here * value_dim)
        * jax.nn.silu(gate_rows)
    ).astype(jnp.bfloat16)
    new_tokens = moe(
        gated_rows,
        tokens,
        norm_gain,
        norm_bias,
        group_router.T,
        routes,
        output_weight,
        router_weight,
        expert_gate,
        expert_up,
        expert_down,
    )
    return (new_tokens, new_state)


def solution(mesh):
    in_specs = (
        P("ep", None),
        P("ep", "tp", None, None),
        P(None, "tp"),
        P(None, "tp"),
        P(None, "tp"),
        P(None, "tp"),
        P(None, "tp"),
        P(),
        P("tp", None),
        P(),
        P(),
        P(),
        P(),
        P("ep", None),
        P(("ep", "tp"), None, None),
        P(("ep", "tp"), None, None),
        P(("ep", "tp"), None, None),
    )
    out_specs = (P("ep", "tp"), P("ep", "tp", None, None))
    return jax.shard_map(
        on_device, mesh=mesh, in_specs=in_specs, out_specs=out_specs, check_vma=False
    )
```

time: 127 us -> 74.6 us (0.59)
  Pallas kernels: 0 us -> 54.8 us
  blocking collectives: 51.6 us -> 0 us
  waiting for transfers between devices: 28.3 us -> 0 us
  matrix products: 15.4 us -> 4.91 us
  starting transfers between devices: 8.22 us -> 0 us
  local copies, waits for them, and re-layouts: 12.9 us -> 7.67 us
  other arithmetic: 9.27 us -> 5.98 us
    pallas_call x0 -> x1, Pallas kernels: none -> 54.8 us  [moe(): pl.pallas_call(moe_kernel, out_shape=jax.ShapeDtypeStruct((ROWS, HALF), B...]
    all_to_all x1 -> x0, blocking collectives: 43.1 us -> none  [on_device(): lax.all_to_all(outgoing, 'ep', split_axis=0, concat_axis=0, tiled=True)]
    all_to_all x1 -> x0, waiting for transfers between devices: 28.3 us -> none  [joined_exchange(): lax.all_to_all(pieces, axis, split_axis=0, concat_axis=0, tiled=True)]
    dot_general x7 -> x0, matrix products: 11.3 us -> none  [the longest x1 3.91 us: on_device(): jnp.einsum('secf,efd->secd', activation, expert_down, preferred_element_t...]
    all_to_all x1 -> x0, starting transfers between devices: 8.22 us -> none  [joined_exchange(): lax.all_to_all(pieces, axis, split_axis=0, concat_axis=0, tiled=True)]
    unnamed x20 -> x33, local copies, waits for them, and re-layouts: 0.81 us -> 7.59 us
    another operation x3 -> x0, local copies, waits for them, and re-layouts: 5.66 us -> none  [the longest x1 2.61 us: joined_exchange(): pieces = jnp.moveaxis(cut_along(pieces, splits[1] + 1, sizes[1]), 0, 1)]
    all_gather x1 -> x0, blocking collectives: 4.74 us -> none  [total_of_pieces(): return lax.all_gather(x, axis).astype(jnp.float32).sum(0)]
  transfers between devices with their start and end apart: 1 -> 0, of which waited for: 1 -> 0; matrix products, arithmetic and copies ran while one was open for 2% -> 0% of each run, Pallas kernels for 0% -> 0%
where the time goes in v1:
time: 74.6 us; the launch traced here: 74.2 us
  Pallas kernels  54.8 us (73%)
  local copies, waits for them, and re-layouts  7.67 us (10%)
  other arithmetic  5.98 us (8%)
  matrix products  4.91 us (7%)
  between operations  0.87 us (1%)
    pallas_call x1, Pallas kernels, moe(): pl.pallas_call(moe_kernel, out_shape=jax.ShapeDtypeStruct((ROWS, HALF), B...  54.8 us
    unnamed x33, local copies, waits for them, and re-layouts  7.59 us
    reduce_sum x1, other arithmetic, on_device(): readout = jnp.sum(queries[..., None] * new_state, axis=2)  5.8 us
    dot_general x5, matrix products, project(): return jnp.dot(tokens, weight, preferred_element_type=jnp.float32)  4.91 us

profile of v1, /device:TPU:1, one launch (start us, length us, event | category | flops | bytes accessed | tf_op | source)
XLA Modules:
  0.0 74.2 jit_solution(11791189612440873352)
XLA Ops:
  0.6 0.0 copy-start
  0.6 0.0 copy-start.1
  0.7 1.6 %copy-done = bf16[2048,512]{1,0:T(8,128)(2,1)S(1)} copy-done((bf16[2048,512]{1,0:T(8,128)(2,1)S(1)}, bf16[2048,512]{1,0:T(8,128)(2,1)}, u32[]{:S(2)}) %copy-start) | copy-done | bytes 2097176
  2.2 1.2 %fusion.4 = f32[16,512]{1,0:T(8,128)S(1)} fusion(bf16[16,2048]{1,0:T(8,128)(2,1)} %tokens_ref.1, bf16[2048,512]{1,0:T(8,128)(2,1)S(1)} %copy-done), kind=kOutput, calls=%fused_computation.14 | convolution fusion | flops 33554432 | bytes 2195456 | tf_op jit(solution)/shard_map/dot_general | solution.py:491
  3.5 1.5 %convolution_multiply_fusion = f32[16,256]{1,0:T(8,128)S(1)} fusion(bf16[16,2048]{1,0:T(8,128)(2,1)} %tokens_ref.1, bf16[2048,256]{1,0:T(8,128)(2,1)} %param.19), kind=kOutput, calls=%fused_computation.3 | convolution fusion | flops 16781312 | bytes 1130496 | tf_op jit(solution)/shard_map/dot_general | solution.py:491
  5.0 1.5 %fusion.2 = f32[16,256]{1,0:T(8,128)S(1)} fusion(bf16[16,2048]{1,0:T(8,128)(2,1)} %tokens_ref.1, bf16[2048,256]{1,0:T(8,128)(2,1)} %param.21), kind=kOutput, calls=%fused_computation.9 | convolution fusion | flops 16814080 | bytes 1130496 | tf_op jit(solution)/shard_map/dot_general | solution.py:491
  6.6 0.2 fusion.3
  6.9 0.0 copy-start.12
  6.9 0.0 copy-start.10
  6.9 0.0 copy-start.13
  6.9 0.0 copy-start.3
  6.9 0.0 copy-start.7
  6.9 0.0 copy-start.8
  6.9 5.8 %multiply_reduce_fusion = (f32[16,2,256]{2,1,0:T(2,128)S(1)}, f32[16,2,128,256]{3,2,1,0:T(8,128)}) fusion(f32[16,2,128]{2,1,0:T(2,128)S(1)} %mul.85, f32[16,2,256]{2,1,0:T(2,128)S(1)} %mul.92, f32[16,2,128]{2,1,0:T(2,128)S(1)} %mul.90, f32[16,2,128,256]{3,2,1,0:T(8,128)} %param.18, f32[16,2,128]{2,1,0:T(2,128)S(1)} %mul.87), kind=kLoop, calls=%fused_computation | loop fusion | flops 5234688 | bytes 8503296 | tf_op jit(solution)/shard_map/reduce_sum | solution.py:503
  12.8 0.1 multiply_reduce_fusion.1
  12.9 0.1 broadcast_multiply_fusion
  13.0 0.4 multiply_convert_fusion.gated_ref
  13.4 0.1 copy.19.routes_ref
  13.5 1.6 %copy-done.2 = bf16[512,2048]{1,0:T(8,128)(2,1)S(1)} copy-done((bf16[512,2048]{1,0:T(8,128)(2,1)S(1)}, bf16[512,2048]{1,0:T(8,128)(2,1)}, u32[]{:S(2)}) %copy-start.2) | copy-done | bytes 2097176
  15.1 1.2 %copy-done.4 = bf16[1,2048,256]{2,1,0:T(8,128)(2,1)S(1)} copy-done((bf16[1,2048,256]{2,1,0:T(8,128)(2,1)S(1)}, bf16[1,2048,256]{2,1,0:T(8,128)(2,1)}, u32[]{:S(2)}) %copy-start.4) | copy-done | bytes 1048600
  16.4 1.2 %copy-done.5 = bf16[1,2048,256]{2,1,0:T(8,128)(2,1)S(1)} copy-done((bf16[1,2048,256]{2,1,0:T(8,128)(2,1)S(1)}, bf16[1,2048,256]{2,1,0:T(8,128)(2,1)}, u32[]{:S(2)}) %copy-start.5) | copy-done | bytes 1048600
  17.6 1.2 %copy-done.6 = bf16[1,256,2048]{2,1,0:T(8,128)(2,1)S(1)} copy-done((bf16[1,256,2048]{2,1,0:T(8,128)(2,1)S(1)}, bf16[1,256,2048]{2,1,0:T(8,128)(2,1)}, u32[]{:S(2)}) %copy-start.6) | copy-done | bytes 1048600
  18.8 54.8 %route_and_experts.1 = bf16[16,1024]{1,0:T(8,128)(2,1)S(1)} custom-call(bf16[16,512]{1,0:T(8,128)(2,1)S(1)} %multiply_convert_fusion.gated_ref, bf16[16,2048]{1,0:T(8,128)(2,1)S(1)} %copy-done.1, f32[2,2048]{1,0:T(2,128)S(1)} %copy-done.7, f32[2,2048]{1,0:T(2,128)S(1)} %copy-done.8, bf16[4,2048]{1,0:T(4,128)(2,1)S(1)} %bitcast.16, ...), custom_call_target="tpu_custom_call" | custom-call | tf_op jit(solution)/shard_map/route_and_experts/pallas_call | solution.py:425
  73.6 0.6 copy.23
  (23 shorter events, 0.1 us)
Async XLA Ops:
  0.6 1.6 %copy-start = (bf16[2048,512]{1,0:T(8,128)(2,1)S(1)}, bf16[2048,512]{1,0:T(8,128)(2,1)}, u32[]{:S(2)}) copy-start(bf16[2048,512]{1,0:T(8,128)(2,1)} %param.22) | copy-start | bytes 6291460
  0.6 5.9 %copy-start.1 = (bf16[16,2048]{1,0:T(8,128)(2,1)S(1)}, bf16[16,2048]{1,0:T(8,128)(2,1)}, u32[]{:S(2)}) copy-start(bf16[16,2048]{1,0:T(8,128)(2,1)} %tokens_ref.1) | copy-start | bytes 196612
  0.7 5.9 %copy-start.11 = (bf16[2048,256]{1,0:T(8,128)(2,1)S(1)}, bf16[2048,256]{1,0:T(8,128)(2,1)}, u32[]{:S(2)}) copy-start(bf16[2048,256]{1,0:T(8,128)(2,1)} %param.20) | copy-start | bytes 3145732
  6.9 6.1 %copy-start.12 = (f32[256]{0:T(256)S(1)}, f32[256]{0:T(256)}, u32[]{:S(2)}) copy-start(f32[256]{0:T(256)} %param.24) | copy-start | bytes 3076
  6.9 6.1 %copy-start.10 = (bf16[2048,512]{1,0:T(8,128)(2,1)S(1)}, bf16[2048,512]{1,0:T(8,128)(2,1)}, u32[]{:S(2)}) copy-start(bf16[2048,512]{1,0:T(8,128)(2,1)} %param.23) | copy-start | bytes 6291460
  6.9 6.5 %copy-start.13 = (s32[16,2]{0,1:T(2,128)S(1)}, s32[16,2]{0,1:T(2,128)}, u32[]{:S(2)}) copy-start(s32[16,2]{0,1:T(2,128)} %param.30) | copy-start | bytes 388
  6.9 6.6 %copy-start.3 = (bf16[2048,256]{1,0:T(8,128)(2,1)S(1)}, bf16[2048,256]{1,0:T(8,128)(2,1)}, u32[]{:S(2)}) copy-start(bf16[2048,256]{1,0:T(8,128)(2,1)} %router_hbm.1) | copy-start | bytes 3145732
  6.9 6.6 %copy-start.7 = (f32[2,2048]{1,0:T(2,128)S(1)}, f32[2,2048]{1,0:T(2,128)}, u32[]{:S(2)}) copy-start(f32[2,2048]{1,0:T(2,128)} %gain_ref.1) | copy-start | bytes 49156
  6.9 6.6 %copy-start.8 = (f32[2,2048]{1,0:T(2,128)S(1)}, f32[2,2048]{1,0:T(2,128)}, u32[]{:S(2)}) copy-start(f32[2,2048]{1,0:T(2,128)} %bias_ref.1) | copy-start | bytes 49156
  6.9 6.6 %copy-start.9 = (bf16[2048,4]{0,1:T(4,128)(2,1)S(1)}, bf16[2048,4]{0,1:T(4,128)(2,1)}, u32[]{:S(2)}) copy-start(bf16[2048,4]{0,1:T(4,128)(2,1)} %param.28) | copy-start | bytes 49156
  13.5 1.6 %copy-start.2 = (bf16[512,2048]{1,0:T(8,128)(2,1)S(1)}, bf16[512,2048]{1,0:T(8,128)(2,1)}, u32[]{:S(2)}) copy-start(bf16[512,2048]{1,0:T(8,128)(2,1)} %wo_hbm.1) | copy-start | bytes 6291460
  15.1 1.2 %copy-start.4 = (bf16[1,2048,256]{2,1,0:T(8,128)(2,1)S(1)}, bf16[1,2048,256]{2,1,0:T(8,128)(2,1)}, u32[]{:S(2)}) copy-start(bf16[1,2048,256]{2,1,0:T(8,128)(2,1)} %gate_hbm.1) | copy-start | bytes 3145732
  16.4 1.2 %copy-start.5 = (bf16[1,2048,256]{2,1,0:T(8,128)(2,1)S(1)}, bf16[1,2048,256]{2,1,0:T(8,128)(2,1)}, u32[]{:S(2)}) copy-start(bf16[1,2048,256]{2,1,0:T(8,128)(2,1)} %up_hbm.1) | copy-start | bytes 3145732
  17.6 1.2 %copy-start.6 = (bf16[1,256,2048]{2,1,0:T(8,128)(2,1)S(1)}, bf16[1,256,2048]{2,1,0:T(8,128)(2,1)}, u32[]{:S(2)}) copy-start(bf16[1,256,2048]{2,1,0:T(8,128)(2,1)} %down_hbm.1) | copy-start | bytes 3145732

commit v2 on v1

--- a/solution.py
+++ b/solution.py
@@ -262,14 +262,7 @@
             arrive[0, h, j].wait_recv()
             p2_sends(h, j)
         half_copies[0, h] = to_pair(slot(0, h, 0), 4)
-    for j in (0, 1, 2, 3):
-        for h in range(2):
-            forward(h, j)
-
     my_expert = lax.rem(ep, 32) * 2 + core
-
-    for load in loads[2:]:
-        load.wait()
 
     def experts(i, count):
         rows = count * 128
@@ -298,10 +291,14 @@
         span = slice(i * 8, (i + count) * 8)
         red[span] = (red[span].astype(F32) + pr[span].astype(F32)).astype(BF16)
 
+    for load in loads[2:]:
+        load.wait()
     for h in range(2):
         half_copies[0, h].wait_recv()
     result0 = experts(0, 1)
-
+    for j in (0, 1, 2, 3):
+        for h in range(2):
+            forward(h, j)
     for i in (1, 2):
         for h in range(2):
             for j in range(4):
@@ -457,10 +454,139 @@
             pltpu.SemaphoreType.DMA((NCOPY,)),
         ],
         compiler_params=pltpu.CompilerParams(
-            collective_id=0, has_side_effects=True, vmem_limit_bytes=40 * 1024 * 1024
+            collective_id=0, has_side_effects=True, vmem_limit_bytes=60 * 1024 * 1024
         ),
         name="route_and_experts",
     )(gated, tokens, gain, bias, group_rows, routes, wo, router, gate, up, down)
+
+
+CHUNK = 2
+NCHUNK = ROWS // CHUNK
+
+
+def attention_kernel(
+    tokens_ref,
+    head_gain_ref,
+    key_hbm,
+    value_hbm,
+    decay_hbm,
+    query_hbm,
+    gate_hbm,
+    state_hbm,
+    gated_ref,
+    new_hbm,
+    key_v,
+    value_v,
+    decay_v,
+    query_v,
+    gate_v,
+    state_v,
+    columns,
+    values,
+    readout,
+    load_sem,
+    in_sem,
+    out_sem,
+):
+    loads = []
+    for n, (src, dst) in enumerate(
+        (
+            (decay_hbm, decay_v),
+            (key_hbm, key_v),
+            (query_hbm, query_v),
+            (value_hbm, value_v),
+        )
+    ):
+        load = pltpu.make_async_copy(src, dst, load_sem.at[n])
+        load.start()
+        loads.append(load)
+    states = []
+    for n in range(NCHUNK):
+        span = pl.ds(n * CHUNK, CHUNK)
+        load = pltpu.make_async_copy(state_hbm.at[span], state_v.at[span], in_sem.at[n])
+        load.start()
+        states.append(load)
+    gate_load = pltpu.make_async_copy(gate_hbm, gate_v, load_sem.at[4])
+    gate_load.start()
+
+    tokens = tokens_ref[...]
+    loads[0].wait()
+    decay = jnp.exp(jax.nn.log_sigmoid(dotf(tokens, decay_v[...])) / 16.0)
+    loads[1].wait()
+    keys = dotf(tokens, key_v[...])
+    loads[2].wait()
+    queries = dotf(tokens, query_v[...]) * 128 ** (-0.5)
+    stacked = jnp.concatenate(
+        [decay, keys, queries, jnp.zeros((128 - 3 * ROWS, 256), F32)], axis=0
+    )
+    columns[...] = stacked.T
+    loads[3].wait()
+    values[...] = dotf(tokens, value_v[...])
+
+    stores = []
+    for n in range(NCHUNK):
+        states[n].wait()
+        for b in range(n * CHUNK, (n + 1) * CHUNK):
+            for h in range(2):
+                rows = slice(h * 128, (h + 1) * 128)
+                decay_col = columns[rows, b : b + 1]
+                key_col = columns[rows, ROWS + b : ROWS + b + 1]
+                query_col = columns[rows, 2 * ROWS + b : 2 * ROWS + b + 1]
+                value_row = values[b : b + 1, h * 256 : (h + 1) * 256]
+                fresh = decay_col * state_v[b, h] + key_col * value_row
+                state_v[b, h] = fresh
+                readout[b : b + 1, h * 256 : (h + 1) * 256] = jnp.sum(
+                    query_col * fresh, axis=0, keepdims=True
+                )
+        span = pl.ds(n * CHUNK, CHUNK)
+        store = pltpu.make_async_copy(state_v.at[span], new_hbm.at[span], out_sem.at[n])
+        store.start()
+        stores.append(store)
+
+    gate_load.wait()
+    gate_rows = dotf(tokens, gate_v[...])
+    for h in range(2):
+        cols = slice(h * 256, (h + 1) * 256)
+        read = readout[:, cols]
+        scale = lax.rsqrt(jnp.mean(read * read, axis=-1, keepdims=True) + EPS)
+        gated_ref[:, cols] = (
+            read * scale * head_gain_ref[...] * jax.nn.silu(gate_rows[:, cols])
+        ).astype(BF16)
+    for store in stores:
+        store.wait()
+
+
+def attention(tokens, head_gain, key_w, value_w, decay_w, query_w, gate_w, state):
+    vmem = pl.BlockSpec(memory_space=pltpu.VMEM)
+    anywhere = pl.BlockSpec(memory_space=pl.ANY)
+    return pl.pallas_call(
+        attention_kernel,
+        out_shape=(
+            jax.ShapeDtypeStruct((ROWS, 512), BF16),
+            jax.ShapeDtypeStruct(state.shape, F32),
+        ),
+        in_specs=[vmem] * 2 + [anywhere] * 6,
+        out_specs=(vmem, anywhere),
+        scratch_shapes=[
+            pltpu.VMEM((WIDTH, 256), BF16),
+            pltpu.VMEM((WIDTH, 512), BF16),
+            pltpu.VMEM((WIDTH, 256), BF16),
+            pltpu.VMEM((WIDTH, 256), BF16),
+            pltpu.VMEM((WIDTH, 512), BF16),
+            pltpu.VMEM((ROWS, 2, 128, 256), F32),
+            pltpu.VMEM((256, 128), F32),
+            pltpu.VMEM((ROWS, 512), F32),
+            pltpu.VMEM((ROWS, 512), F32),
+            pltpu.SemaphoreType.DMA((5,)),
+            pltpu.SemaphoreType.DMA((NCHUNK,)),
+            pltpu.SemaphoreType.DMA((NCHUNK,)),
+        ],
+        compiler_params=pltpu.CompilerParams(vmem_limit_bytes=60 * 1024 * 1024),
+        cost_estimate=pl.CostEstimate(
+            flops=150_000_000, bytes_accessed=15_000_000, transcendentals=10_000
+        ),
+        name="attention_state",
+    )(tokens, head_gain, key_w, value_w, decay_w, query_w, gate_w, state)
 
 
 def on_device(
@@ -482,30 +608,16 @@
     expert_up,
     expert_down,
 ):
-    row_count, model_width = tokens.shape
-    heads_here = recurrent_state.shape[1]
-    key_dim = recurrent_state.shape[2]
-    value_dim = recurrent_state.shape[3]
-
-    def project(weight):
-        return jnp.dot(tokens, weight, preferred_element_type=jnp.float32)
-
-    queries = project(query_weight).reshape(row_count, heads_here, key_dim) * key_dim ** (-0.5)
-    key_rows = project(key_weight).reshape(row_count, heads_here, key_dim)
-    value_rows = project(value_weight).reshape(row_count, heads_here, value_dim)
-    gate_rows = project(gate_weight)
-    decay_rate = jnp.exp(jax.nn.log_sigmoid(project(decay_weight)) / 16.0).reshape(
-        row_count, heads_here, key_dim
+    gated_rows, new_state = attention(
+        tokens,
+        head_gain.reshape(1, 256),
+        key_weight,
+        value_weight,
+        decay_weight,
+        query_weight,
+        gate_weight,
+        recurrent_state,
     )
-    new_state = (
-        decay_rate[..., None] * recurrent_state + key_rows[..., None] * value_rows[:, :, None, :]
-    )
-    readout = jnp.sum(queries[..., None] * new_state, axis=2)
-    norm_scale = lax.rsqrt(jnp.mean(readout * readout, axis=-1, keepdims=True) + EPS)
-    gated_rows = (
-        (readout * norm_scale * head_gain).reshape(row_count, heads_here * value_dim)
-        * jax.nn.silu(gate_rows)
-    ).astype(jnp.bfloat16)
     new_tokens = moe(
         gated_rows,
         tokens,

time: 74.6 us -> 67.7 us (0.908)
  Pallas kernels: 54.8 us -> 64.1 us
  other arithmetic: 5.98 us -> 0 us
  local copies, waits for them, and re-layouts: 7.67 us -> 2.73 us
  matrix products: 4.91 us -> 0 us
    pallas_call x0 -> x1, Pallas kernels: none -> 8.69 us  [attention(): pl.pallas_call(attention_kernel, out_shape=(jax.ShapeDtypeStruct((ROWS, 5...]
    reduce_sum x2 -> x0, other arithmetic: 5.89 us -> none  [the longest x1 5.8 us: on_device(): readout = jnp.sum(queries[..., None] * new_state, axis=2)]
    dot_general x5 -> x0, matrix products: 4.91 us -> none  [project(): return jnp.dot(tokens, weight, preferred_element_type=jnp.float32)]
    unnamed x33 -> x2, local copies, waits for them, and re-layouts: 7.59 us -> 2.73 us
where the time goes in v2:
time: 67.7 us; the launch traced here: 67.4 us
  Pallas kernels  64.1 us (95%)
  local copies, waits for them, and re-layouts  2.73 us (4%)
    pallas_call x1, Pallas kernels, moe(): pl.pallas_call(moe_kernel, out_shape=jax.ShapeDtypeStruct((ROWS, HALF), B...  55.4 us
    pallas_call x1, Pallas kernels, attention(): pl.pallas_call(attention_kernel, out_shape=(jax.ShapeDtypeStruct((ROWS, 5...  8.69 us
    unnamed x2, local copies, waits for them, and re-layouts  2.73 us

profile of v2, /device:TPU:1, one launch (start us, length us, event | category | flops | bytes accessed | tf_op | source)
XLA Modules:
  0.0 67.4 jit_solution(4680780624250935320)
XLA Ops:
  0.6 1.4 %copy.19.routes_ref = s32[16,2]{1,0:T(8,128)} copy(s32[16,2]{0,1:T(2,128)} %param.30) | data formatting | bytes 256 | tf_op args[13]
  2.0 8.7 %attention_state.1 = (bf16[16,512]{1,0:T(8,128)(2,1)}, f32[16,2,128,256]{3,2,1,0:T(8,128)}) custom-call(bf16[16,2048]{1,0:T(8,128)(2,1)} %tokens_ref.3, f32[1,256]{1,0:T(1,128)} %bitcast.3, bf16[2048,256]{1,0:T(8,128)(2,1)} %key_hbm.1, bf16[2048,512]{1,0:T(8,128)(2,1)} %value_hbm.1, bf16[2048,256]{1,0:T(8,128)(2,1)} %decay_hbm.1, ...), custom_call_target="tpu_custom_call" | custom-call | flops 150000000 | bytes 15000000 | tf_op jit(solution)/shard_map/attention_state/pallas_call | solution.py:562
  10.7 55.4 %route_and_experts.1 = bf16[16,1024]{1,0:T(8,128)(2,1)} custom-call(bf16[16,512]{1,0:T(8,128)(2,1)} %get-tuple-element.4.gated_ref, bf16[16,2048]{1,0:T(8,128)(2,1)} %tokens_ref.3, f32[2,2048]{1,0:T(2,128)} %gain_ref.1, f32[2,2048]{1,0:T(2,128)} %bias_ref.1, bf16[4,2048]{1,0:T(4,128)(2,1)} %bitcast.2, s32[16,2]{1,0:T(8,128)} %copy.19.routes_ref, ...), custom_call_target="tpu_custom_call" | custom-call | tf_op jit(solution)/shard_map/route_and_experts/pallas_call | solution.py:422
  66.1 1.4 %copy.21 = bf16[16,1024]{1,0:T(8,128)(2,1)} copy(bf16[16,1024]{1,0:T(8,128)(2,1)} %route_and_experts.1) | data formatting | bytes 65536
